TPU v7x, 32 devices: a whole 2x2x4 slice. The times are simulated.
32 devices in a mesh: fs: 8 (over z, y), tp: 4 (over x, core).
Axes of the slice: x: 2, y: 2, z: 4, core: 2. Of those that a mesh axis runs over, the one named last changes fastest.
Arguments:
- tokens: bfloat16 [3072, 2048], P('fs'), may hold values from -6 to 6
- first_norm_scale: float32 [2048], replicated, may hold values from 0.1 to 1.9
- recurrent_branch_matrix: bfloat16 [2048, 1024], P('fs', 'tp'), may hold values from -0.125 to 0.125
- gelu_gate_matrix: bfloat16 [2048, 1024], P('fs', 'tp'), may hold values from -0.125 to 0.125
- filter_taps_weight: bfloat16 [4, 1024], P(None, 'tp'), may hold values from -3 to 3
- recurrence_gate_blocks: bfloat16 [16, 64, 64], P('tp'), may hold values from -0.75 to 0.75
- input_gate_blocks: bfloat16 [16, 64, 64], P('tp'), may hold values from -0.75 to 0.75
- base_decay_logits: float32 [1024], P('tp'), may hold values from 4 to 11
- extra_log_decay: float32 [3072, 1024], P('fs', 'tp'), may hold values from -0.7 to 0
- mixer_output_matrix: bfloat16 [2048, 1024], P('fs', 'tp'), may hold values from -0.5 to 0.5
- second_norm_scale: float32 [2048], replicated, may hold values from 0.1 to 1.9
- mixer_up_matrix: bfloat16 [2048, 4096], P('fs', 'tp'), may hold values from -0.125 to 0.125
- mixer_down_matrix: bfloat16 [2048, 4096], P('fs', 'tp'), may hold values from -0.09375 to 0.09375
Outputs:
- layer_out: bfloat16 [3072, 2048], P(('fs', 'tp'))
All inputs are finite; a program needn't handle non-finite values.
Results may differ from a plain program's by a relative error of at most 0.022.
Values may be sent and summed in bfloat16 or wider, within the bound.
A program may use at most 64 MiB of HBM per device.

v0:
```python
import jax
import jax.numpy as jnp
from jax import lax
from jax.sharding import PartitionSpec as P

epsilon = 1e-06
decay_rate_scale = 8.0


def rms_scaled(sequence_token_rows, scales):
    widened = sequence_token_rows.astype(jnp.float32)
    mean_square = jnp.mean(widened * widened, axis=-1, keepdims=True)
    return (widened * lax.rsqrt(mean_square + epsilon) * scales).astype(jnp.bfloat16)


def linear_combine(earlier, later):
    return (earlier[0] * later[0], later[0] * earlier[1] + later[1])


def causal_taps(branch, filter_taps_weight):
    tap_count = filter_taps_weight.shape[0]
    positions = branch.shape[0]
    padded = jnp.pad(branch.astype(jnp.float32), ((tap_count - 1, 0), (0, 0)))
    running = jnp.zeros(branch.shape, jnp.float32)
    for offset in range(tap_count):
        running = running + padded[offset : offset + positions] * filter_taps_weight[offset].astype(
            jnp.float32
        )
    return running.astype(jnp.bfloat16)


def block_map(convolved, blocks):
    positions, channels = convolved.shape
    grouped = convolved.reshape(positions, blocks.shape[0], blocks.shape[1])
    mapped = jnp.einsum("sgi,gij->sgj", grouped, blocks, preferred_element_type=jnp.float32)
    return jax.nn.sigmoid(mapped.reshape(positions, channels))


def contract_columns(left, right):
    return lax.dot_general(
        left, right, (((1,), (1,)), ((), ())), preferred_element_type=jnp.float32
    )


def local(
    tokens,
    first_norm_scale,
    recurrent_branch_matrix,
    gelu_gate_matrix,
    filter_taps_weight,
    recurrence_gate_blocks,
    input_gate_blocks,
    base_decay_logits,
    extra_log_decay,
    mixer_output_matrix,
    second_norm_scale,
    mixer_up_matrix,
    mixer_down_matrix,
):
    positions = tokens.shape[0]
    own_count = positions // lax.axis_size("tp")
    normed = rms_scaled(tokens, first_norm_scale)
    branch_sum = jnp.dot(
        normed,
        lax.all_gather(recurrent_branch_matrix, "fs", axis=0, tiled=True),
        preferred_element_type=jnp.float32,
    )
    gate_sum = jnp.dot(
        normed,
        lax.all_gather(gelu_gate_matrix, "fs", axis=0, tiled=True),
        preferred_element_type=jnp.float32,
    )
    branch = branch_sum.astype(jnp.bfloat16)
    gate_branch = gate_sum.astype(jnp.bfloat16)
    out_full = lax.all_gather(mixer_output_matrix, "fs", axis=0, tiled=True)
    convolved = causal_taps(branch, filter_taps_weight)
    recurrence_gate_value = block_map(convolved, recurrence_gate_blocks)
    admission = block_map(convolved, input_gate_blocks)
    log_keep_factor = (
        decay_rate_scale * recurrence_gate_value * jax.nn.log_sigmoid(base_decay_logits)
        + extra_log_decay
    )
    retain = jnp.exp(log_keep_factor)
    driven = jnp.sqrt(-jnp.expm1(2.0 * log_keep_factor)) * (
        admission * convolved.astype(jnp.float32)
    )
    memory = lax.associative_scan(linear_combine, (retain, driven), axis=0)[1]
    recurrent = (memory * jax.nn.gelu(gate_branch.astype(jnp.float32))).astype(jnp.bfloat16)
    up_full = lax.all_gather(mixer_up_matrix, "fs", axis=0, tiled=True)
    whole_sum = lax.psum(contract_columns(recurrent, out_full).astype(jnp.bfloat16), "tp").astype(
        jnp.float32
    )
    residual_all = (tokens.astype(jnp.float32) + whole_sum).astype(jnp.bfloat16)
    raised = jnp.dot(
        rms_scaled(residual_all, second_norm_scale), up_full, preferred_element_type=jnp.float32
    )
    hidden = jnp.square(jax.nn.relu(raised)).astype(jnp.bfloat16)
    residual = lax.dynamic_slice_in_dim(
        residual_all, lax.axis_index("tp") * own_count, own_count, 0
    )
    down_full = lax.all_gather(mixer_down_matrix, "fs", axis=0, tiled=True)
    channel_sum = lax.psum_scatter(
        contract_columns(hidden, down_full).astype(jnp.bfloat16),
        "tp",
        scatter_dimension=0,
        tiled=True,
    ).astype(jnp.float32)
    return (residual.astype(jnp.float32) + channel_sum).astype(jnp.bfloat16)


def solution(mesh):
    in_specs = (
        P("fs", None),
        P(),
        P("fs", "tp"),
        P("fs", "tp"),
        P(None, "tp"),
        P("tp", None, None),
        P("tp", None, None),
        P("tp"),
        P("fs", "tp"),
        P("fs", "tp"),
        P(),
        P("fs", "tp"),
        P("fs", "tp"),
    )
    out_specs = P(("fs", "tp"), None)
    return jax.shard_map(local, mesh=mesh, in_specs=in_specs, out_specs=out_specs, check_vma=False)
```

profile of v0, /device:TPU:0, one launch (start us, length us, event | category | flops | bytes accessed | tf_op | source)
XLA Modules:
  0.0 372.9 jit_solution(10167174261476025850)
XLA Ops:
  6.5 0.7 all-gather.6.cloned.1.call-update
  7.3 0.7 all-gather.10.cloned.1.call-update
  8.1 0.7 all-gather.8.cloned.1.call-update
  8.8 0.8 slice_convert_fusion.3
  9.6 1.8 fusion.3
  11.4 0.7 fusion.59
  12.1 40.4 %all-gather.6.cloned.1.call-done = bf16[2048,256]{1,0:T(8,128)(2,1)} async-done(((bf16[256,256]{1,0:T(8,128)(2,1)}), bf16[2048,256]{1,0:T(8,128)(2,1)}) %all-gather.6.cloned.1.call-update) | async-done | bytes 1048592 | tf_op jit(solution)/shard_map/all_gather | solution.py:65
  52.5 2.3 fusion.20
  55.2 0.3 fusion.18
  55.7 0.3 fusion.15
  56.2 0.5 fusion.49
  58.3 0.3 slice.278
  59.8 33.8 %all-gather.10.cloned.1.call-done = bf16[2048,256]{1,0:T(8,128)(2,1)} async-done(((bf16[256,256]{1,0:T(8,128)(2,1)}), bf16[2048,256]{1,0:T(8,128)(2,1)}) %all-gather.10.cloned.1.call-update) | async-done | bytes 1048592 | tf_op jit(solution)/shard_map/all_gather | solution.py:75
  93.6 41.2 %all-gather.8.cloned.1.call-done = bf16[2048,256]{1,0:T(8,128)(2,1)} async-done(((bf16[256,256]{1,0:T(8,128)(2,1)}), bf16[2048,256]{1,0:T(8,128)(2,1)}) %all-gather.8.cloned.1.call-update) | async-done | bytes 1048592 | tf_op jit(solution)/shard_map/all_gather | solution.py:70
  134.8 4.6 %convolution_convert_fusion.1 = bf16[384,2048]{1,0:T(8,128)(2,1)} fusion(bf16[2048,256]{1,0:T(8,128)(2,1)} %all-gather.10.cloned.1.call-done, bf16[2048,256]{1,0:T(8,128)(2,1)} %all-gather.8.cloned.1.call-done, bf16[384,2048]{1,0:T(8,128)(2,1)S(1)} %copy-done.1, f32[2048]{0:T(1024)S(1)} %copy-done.4, f32[384]{0:T(512)S(1)} %add_rsqrt_fusion.1, ...), kind=kOutput, calls=%fused_computation.13 | convolution fusion | flops 810516480 | bytes 6039040 | tf_op jit(solution)/shard_map/dot_general | solution.py:40
  139.5 0.5 all-gather.12.cloned.1.call-update
  140.1 0.5 all-gather.14.cloned.1.call-update
  140.7 40.5 %all-reduce.19.cloned.1.call-done = bf16[384,2048]{1,0:T(8,128)(2,1)} async-done(((bf16[384,2048]{1,0:T(8,128)(2,1)}), bf16[384,2048]{1,0:T(8,128)(2,1)}) %all-reduce.19.cloned.1.call-update) | async-done | bytes 1572880 | tf_op jit(solution)/shard_map/psum | solution.py:90
  181.2 2.1 fusion
  183.3 72.7 %all-gather.12.cloned.1.call-done = bf16[2048,1024]{1,0:T(8,128)(2,1)} async-done(((bf16[256,1024]{1,0:T(8,128)(2,1)}), bf16[2048,1024]{1,0:T(8,128)(2,1)}) %all-gather.12.cloned.1.call-update) | async-done | bytes 4194320 | tf_op jit(solution)/shard_map/all_gather | solution.py:89
  256.0 73.3 %all-gather.14.cloned.1.call-done = bf16[2048,1024]{1,0:T(8,128)(2,1)} async-done(((bf16[256,1024]{1,0:T(8,128)(2,1)}), bf16[2048,1024]{1,0:T(8,128)(2,1)}) %all-gather.14.cloned.1.call-update) | async-done | bytes 4194320 | tf_op jit(solution)/shard_map/all_gather | solution.py:101
  329.4 8.1 %convolution_convert_fusion = bf16[384,2048]{1,0:T(8,128)(2,1)} fusion(bf16[2048,1024]{1,0:T(8,128)(2,1)} %all-gather.14.cloned.1.call-done, bf16[2048,1024]{1,0:T(8,128)(2,1)} %all-gather.12.cloned.1.call-done, bf16[384,2048]{1,0:T(8,128)(2,1)S(1)} %get-tuple-element.6, f32[2048]{0:T(1024)S(1)} %copy-done.5, f32[384]{0:T(512)S(1)} %add_rsqrt_fusion), kind=kOutput, calls=%fused_computation.12 | convolution fusion | flops 3226337280 | bytes 11544064 | tf_op jit(solution)/shard_map/dot_general | solution.py:40
  337.6 26.7 %reduce-scatter.2.cloned.1.call-done = bf16[96,2048]{1,0:T(8,128)(2,1)} async-done(((bf16[384,2048]{1,0:T(8,128)(2,1)}), bf16[96,2048]{1,0:T(8,128)(2,1)}) %reduce-scatter.2.cloned.1.call-update) | async-done | bytes 393232 | tf_op jit(solution)/shard_map/reduce_scatter | solution.py:102
  364.2 1.8 add_convert_fusion
  (120 shorter events, 3.3 us)
Async XLA Ops:
  6.5 48.7 %copy-start = (bf16[4,64,64]{2,1,0:T(8,128)(2,1)S(1)}, bf16[4,64,64]{2,1,0:T(8,128)(2,1)}, u32[]{:S(2)}) copy-start(bf16[4,64,64]{2,1,0:T(8,128)(2,1)} %param.18) | copy-start | bytes 98308
  6.5 46.0 %all-gather.6.cloned.1.call-start = ((), (), s32[]{:S(2)}) async-start(), calls=%async_computation.1 | async-start | bytes 1179648 | tf_op jit(solution)/shard_map/all_gather | solution.py:65
  7.3 86.4 %all-gather.10.cloned.1.call-start = ((), (), s32[]{:S(2)}) async-start(), calls=%async_computation.3 | async-start | bytes 1179648 | tf_op jit(solution)/shard_map/all_gather | solution.py:75
  8.0 126.8 %all-gather.8.cloned.1.call-start = ((), (), s32[]{:S(2)}) async-start(), calls=%async_computation.2 | async-start | bytes 1179648 | tf_op jit(solution)/shard_map/all_gather | solution.py:70
  8.7 172.4 %all-reduce.19.cloned.1.call-start = ((), (), s32[]{:S(2)}) async-start(), calls=%async_computation.4 | async-start | bytes 3145728 | tf_op jit(solution)/shard_map/psum | solution.py:90
  12.1 43.6 %copy-start.3 = (bf16[4,64,64]{2,1,0:T(8,128)(2,1)S(1)}, bf16[4,64,64]{2,1,0:T(8,128)(2,1)}, u32[]{:S(2)}) copy-start(bf16[4,64,64]{2,1,0:T(8,128)(2,1)} %param.19) | copy-start | bytes 98308
  54.8 1.4 copy-start.2
  59.1 75.7 %copy-start.1 = (bf16[384,2048]{1,0:T(8,128)(2,1)S(1)}, bf16[384,2048]{1,0:T(8,128)(2,1)}, u32[]{:S(2)}) copy-start(bf16[384,2048]{1,0:T(8,128)(2,1)} %param.13) | copy-start | bytes 4718596
  59.1 75.7 %copy-start.4 = (f32[2048]{0:T(1024)S(1)}, f32[2048]{0:T(1024)}, u32[]{:S(2)}) copy-start(f32[2048]{0:T(1024)} %param.14) | copy-start | bytes 24580
  139.5 189.9 %copy-start.5 = (f32[2048]{0:T(1024)S(1)}, f32[2048]{0:T(1024)}, u32[]{:S(2)}) copy-start(f32[2048]{0:T(1024)} %param.23) | copy-start | bytes 24580
  139.5 116.6 %all-gather.12.cloned.1.call-start = ((), (), s32[]{:S(2)}) async-start(), calls=%async_computation.5 | async-start | bytes 4718592 | tf_op jit(solution)/shard_map/all_gather | solution.py:89
  140.1 189.3 %all-gather.14.cloned.1.call-start = ((), (), s32[]{:S(2)}) async-start(), calls=%async_computation.6 | async-start | bytes 4718592 | tf_op jit(solution)/shard_map/all_gather | solution.py:101
  140.6 223.6 %reduce-scatter.2.cloned.1.call-start = ((), (), s32[]{:S(2)}) async-start(), calls=%async_computation.7 | async-start | bytes 1966080 | tf_op jit(solution)/shard_map/reduce_scatter | solution.py:102
Sparse Core Ops, SparseCore 0:
  9.5 42.9 all-gather.5
  54.6 38.9 all-gather.9
  95.8 38.9 all-gather.7
  139.6 41.5 all-reduce.18
  183.2 72.8 all-gather.11
  258.0 71.3 all-gather.13
  337.7 26.5 reduce-scatter.1
where the time goes:
time: 373 us
  waiting for transfers between devices  332 us (89%)
  matrix products  15.7 us (4%)
  between operations  14.1 us (4%)
  other arithmetic  8.42 us (2%)
    all_gather x1, waiting for transfers between devices, local(): down_full = lax.all_gather(mixer_down_matrix, 'fs', axis=0, tiled=True)  73.3 us
    all_gather x1, waiting for transfers between devices, local(): up_full = lax.all_gather(mixer_up_matrix, 'fs', axis=0, tiled=True)  72.7 us
    all_gather x1, waiting for transfers between devices, local(): lax.all_gather(gelu_gate_matrix, 'fs', axis=0, tiled=True)  41.2 us
    psum x1, waiting for transfers between devices, local(): lax.psum(contract_columns(recurrent, out_full).astype(jnp.bfloat16), 'tp')  40.5 us
    all_gather x1, waiting for transfers between devices, local(): lax.all_gather(recurrent_branch_matrix, 'fs', axis=0, tiled=True)  40.4 us
    all_gather x1, waiting for transfers between devices, local(): out_full = lax.all_gather(mixer_output_matrix, 'fs', axis=0, tiled=True)  33.8 us
    reduce_scatter x1, waiting for transfers between devices, local(): lax.psum_scatter(contract_columns(hidden, down_full).astype(jnp.bfloat16)...  26.7 us
    dot_general x2, matrix products, contract_columns(): lax.dot_general(left, right, (((1,), (1,)), ((), ())), preferred_element_...  12.8 us
  transfers between devices with their start and end apart: 7, of which 7 were waited for; matrix products, arithmetic and copies ran while one was open for 3% of the time, Pallas kernels for 0%

commit v1 on v0

--- a/solution.py
+++ b/solution.py
@@ -98,7 +98,12 @@
     residual = lax.dynamic_slice_in_dim(
         residual_all, lax.axis_index("tp") * own_count, own_count, 0
     )
-    down_full = lax.all_gather(mixer_down_matrix, "fs", axis=0, tiled=True)
+    ring = [mixer_down_matrix]
+    for hop in range(7):
+        ring.append(lax.ppermute(ring[-1], "fs", [(dev, (dev + 1) % 8) for dev in range(8)]))
+    down_full = jnp.roll(
+        jnp.concatenate(ring[::-1], axis=0), (lax.axis_index("fs") + 1) * ring[0].shape[0], axis=0
+    )
     channel_sum = lax.psum_scatter(
         contract_columns(hidden, down_full).astype(jnp.bfloat16),
         "tp",

time: 373 us -> 330 us (0.88)
  waiting for transfers between devices: 332 us -> 265 us
  local copies, waits for them, and re-layouts: 2.7 us -> 25.9 us
    ppermute x0 -> x7, waiting for transfers between devices: none -> 121 us  [local(): lax.ppermute(ring[-1], 'fs', [(dev, (dev + 1) % 8) for dev in range(8)])]
    all_gather x1 -> x0, waiting for transfers between devices: 73.3 us -> none  [local(): down_full = lax.all_gather(mixer_down_matrix, 'fs', axis=0, tiled=True)]
    all_gather x1, waiting for transfers between devices: 72.7 us -> 0.01 us  [local(): up_full = lax.all_gather(mixer_up_matrix, 'fs', axis=0, tiled=True)]
    psum x1, waiting for transfers between devices: 40.5 us -> 0.01 us  [local(): lax.psum(contract_columns(recurrent, out_full).astype(jnp.bfloat16), 'tp')]
    unnamed x12 -> x51, local copies, waits for them, and re-layouts: 0.03 us -> 22.4 us
  transfers between devices with their start and end apart: 7 -> 13, of which waited for: 7 -> 11; matrix products, arithmetic and copies ran while one was open for 3% -> 10% of each run, Pallas kernels for 0% -> 0%
where the time goes in v1:
time: 330 us
  waiting for transfers between devices  265 us (80%)
  local copies, waits for them, and re-layouts  25.9 us (8%)
  matrix products  15.7 us (5%)
  between operations  14.2 us (4%)
  other arithmetic  8.5 us (3%)
    ppermute x7, waiting for transfers between devices, local(): lax.ppermute(ring[-1], 'fs', [(dev, (dev + 1) % 8) for dev in range(8)])  121 us
    all_gather x1, waiting for transfers between devices, local(): lax.all_gather(gelu_gate_matrix, 'fs', axis=0, tiled=True)  41.2 us
    all_gather x1, waiting for transfers between devices, local(): lax.all_gather(recurrent_branch_matrix, 'fs', axis=0, tiled=True)  40.4 us
    all_gather x1, waiting for transfers between devices, local(): out_full = lax.all_gather(mixer_output_matrix, 'fs', axis=0, tiled=True)  33.8 us
    reduce_scatter x1, waiting for transfers between devices, local(): lax.psum_scatter(contract_columns(hidden, down_full).astype(jnp.bfloat16)...  25.4 us
    unnamed x51, local copies, waits for them, and re-layouts  22.4 us
    dot_general x2, matrix products, contract_columns(): lax.dot_general(left, right, (((1,), (1,)), ((), ())), preferred_element_...  12.7 us
  transfers between devices with their start and end apart: 13, of which 11 were waited for; matrix products, arithmetic and copies ran while one was open for 10% of the time, Pallas kernels for 0%

profile of v1, /device:TPU:0, one launch (start us, length us, event | category | flops | bytes accessed | tf_op | source)
XLA Modules:
  0.0 329.7 jit_solution(18319271848752192857)
XLA Ops:
  8.8 1.8 fusion.5
  12.1 40.4 %all-gather.5.cloned.1.call-done = bf16[2048,256]{1,0:T(8,128)(2,1)} async-done(((bf16[256,256]{1,0:T(8,128)(2,1)}), bf16[2048,256]{1,0:T(8,128)(2,1)}) %all-gather.5.cloned.1.call-update) | async-done | bytes 1048592 | tf_op jit(solution)/shard_map/all_gather | solution.py:65
  52.5 2.3 fusion.25
  59.8 33.8 %all-gather.9.cloned.1.call-done = bf16[2048,256]{1,0:T(8,128)(2,1)} async-done(((bf16[256,256]{1,0:T(8,128)(2,1)}), bf16[2048,256]{1,0:T(8,128)(2,1)}) %all-gather.9.cloned.1.call-update) | async-done | bytes 1048592 | tf_op jit(solution)/shard_map/all_gather | solution.py:75
  93.6 41.2 %all-gather.7.cloned.1.call-done = bf16[2048,256]{1,0:T(8,128)(2,1)} async-done(((bf16[256,256]{1,0:T(8,128)(2,1)}), bf16[2048,256]{1,0:T(8,128)(2,1)}) %all-gather.7.cloned.1.call-update) | async-done | bytes 1048592 | tf_op jit(solution)/shard_map/all_gather | solution.py:70
  134.8 4.6 %convolution_convert_fusion = bf16[384,2048]{1,0:T(8,128)(2,1)} fusion(bf16[2048,256]{1,0:T(8,128)(2,1)} %all-gather.9.cloned.1.call-done, bf16[2048,256]{1,0:T(8,128)(2,1)} %all-gather.7.cloned.1.call-done, bf16[384,2048]{1,0:T(8,128)(2,1)S(1)} %copy-done.1, f32[2048]{0:T(1024)S(1)} %copy-done.16, f32[384]{0:T(512)S(1)} %add_rsqrt_fusion.1, ...), kind=kOutput, calls=%fused_computation.15 | convolution fusion | flops 810516480 | bytes 6039040 | tf_op jit(solution)/shard_map/dot_general | solution.py:40
  140.7 14.1 %collective-permute-done = bf16[256,1024]{1,0:T(8,128)(2,1)S(1)} collective-permute-done((bf16[256,1024]{1,0:T(8,128)(2,1)S(1)}, bf16[256,1024]{1,0:T(8,128)(2,1)S(1)}, u32[]{:S(2)}, u32[]{:S(2)}) %collective-permute-start) | collective-permute-done | bytes 524320 | tf_op jit(solution)/shard_map/ppermute | solution.py:103
  155.6 13.8 %collective-permute-done.1 = bf16[256,1024]{1,0:T(8,128)(2,1)S(1)} collective-permute-done((bf16[256,1024]{1,0:T(8,128)(2,1)S(1)}, bf16[256,1024]{1,0:T(8,128)(2,1)S(1)}, u32[]{:S(2)}, u32[]{:S(2)}) %collective-permute-start.1) | collective-permute-done | bytes 524320 | tf_op jit(solution)/shard_map/ppermute | solution.py:103
  170.2 12.9 %collective-permute-done.2 = bf16[256,1024]{1,0:T(8,128)(2,1)S(1)} collective-permute-done((bf16[256,1024]{1,0:T(8,128)(2,1)S(1)}, bf16[256,1024]{1,0:T(8,128)(2,1)S(1)}, u32[]{:S(2)}, u32[]{:S(2)}) %collective-permute-start.2) | collective-permute-done | bytes 524320 | tf_op jit(solution)/shard_map/ppermute | solution.py:103
  184.0 12.2 %collective-permute-done.3 = bf16[256,1024]{1,0:T(8,128)(2,1)S(1)} collective-permute-done((bf16[256,1024]{1,0:T(8,128)(2,1)S(1)}, bf16[256,1024]{1,0:T(8,128)(2,1)S(1)}, u32[]{:S(2)}, u32[]{:S(2)}) %collective-permute-start.3) | collective-permute-done | bytes 524320 | tf_op jit(solution)/shard_map/ppermute | solution.py:103
  197.0 26.9 %collective-permute-done.4 = bf16[256,1024]{1,0:T(8,128)(2,1)S(1)} collective-permute-done((bf16[256,1024]{1,0:T(8,128)(2,1)S(1)}, bf16[256,1024]{1,0:T(8,128)(2,1)S(1)}, u32[]{:S(2)}, u32[]{:S(2)}) %collective-permute-start.4) | collective-permute-done | bytes 524320 | tf_op jit(solution)/shard_map/ppermute | solution.py:103
  223.9 18.0 %collective-permute-done.5 = bf16[256,1024]{1,0:T(8,128)(2,1)} collective-permute-done((bf16[256,1024]{1,0:T(8,128)(2,1)S(1)}, bf16[256,1024]{1,0:T(8,128)(2,1)}, u32[]{:S(2)}, u32[]{:S(2)}) %collective-permute-start.5) | collective-permute-done | bytes 524320 | tf_op jit(solution)/shard_map/ppermute | solution.py:103
  242.0 2.2 fusion.2
  244.3 23.3 %collective-permute-done.6 = bf16[256,1024]{1,0:T(8,128)(2,1)} collective-permute-done((bf16[256,1024]{1,0:T(8,128)(2,1)}, bf16[256,1024]{1,0:T(8,128)(2,1)}, u32[]{:S(2)}, u32[]{:S(2)}) %collective-permute-start.6) | collective-permute-done | bytes 524320 | tf_op jit(solution)/shard_map/ppermute | solution.py:103
  267.6 1.9 constant_dynamic-update-slice_fusion.15
  269.4 1.9 constant_dynamic-update-slice_fusion.14
  273.0 1.9 constant_dynamic-update-slice_fusion.11
  275.0 2.0 constant_dynamic-update-slice_fusion.10
  278.6 1.9 constant_dynamic-update-slice_fusion.7
  280.5 1.9 constant_dynamic-update-slice_fusion.6
  285.7 0.9 constant_dynamic-update-slice_fusion.1
  287.5 8.1 %fusion.9 = bf16[384,2048]{1,0:T(8,128)(2,1)} fusion(bf16[4096,1024]{1,0:T(8,128)(2,1)} %constant_dynamic-update-slice_fusion, s32[]{:T(128)S(6)} %select_n.24, bf16[2048,1024]{1,0:T(8,128)(2,1)} %all-gather.11.cloned.1.call-done, bf16[384,2048]{1,0:T(8,128)(2,1)S(1)} %get-tuple-element.6, f32[2048]{0:T(1024)S(1)} %copy-done.17, f32[384]{0:T(512)S(1)} %add_rsqrt_fusion), kind=kOutput, calls=%fused_computation.14 | convolution fusion | flops 3226337280 | bytes 11544068 | tf_op jit(solution)/shard_map/dot_general | solution.py:40
  295.6 25.4 %reduce-scatter.2.cloned.1.call-done = bf16[96,2048]{1,0:T(8,128)(2,1)} async-done(((bf16[384,2048]{1,0:T(8,128)(2,1)}), bf16[96,2048]{1,0:T(8,128)(2,1)}) %reduce-scatter.2.cloned.1.call-update) | async-done | bytes 393232 | tf_op jit(solution)/shard_map/reduce_scatter | solution.py:107
  321.0 1.8 add_convert_fusion
  (171 shorter events, 20.3 us)
Async XLA Ops:
  6.5 48.7 %copy-start = (bf16[4,64,64]{2,1,0:T(8,128)(2,1)S(1)}, bf16[4,64,64]{2,1,0:T(8,128)(2,1)}, u32[]{:S(2)}) copy-start(bf16[4,64,64]{2,1,0:T(8,128)(2,1)} %param.18) | copy-start | bytes 98308
  6.5 46.0 %all-gather.5.cloned.1.call-start = ((), (), s32[]{:S(2)}) async-start(), calls=%async_computation.1 | async-start | bytes 1179648 | tf_op jit(solution)/shard_map/all_gather | solution.py:65
  7.3 86.4 %all-gather.9.cloned.1.call-start = ((), (), s32[]{:S(2)}) async-start(), calls=%async_computation.3 | async-start | bytes 1179648 | tf_op jit(solution)/shard_map/all_gather | solution.py:75
  8.0 126.8 %all-gather.7.cloned.1.call-start = ((), (), s32[]{:S(2)}) async-start(), calls=%async_computation.2 | async-start | bytes 1179648 | tf_op jit(solution)/shard_map/all_gather | solution.py:70
  8.7 233.2 %all-reduce.19.cloned.1.call-start = ((), (), s32[]{:S(2)}) async-start(), calls=%async_computation.4 | async-start | bytes 3145728 | tf_op jit(solution)/shard_map/psum | solution.py:90
  10.6 45.1 %copy-start.15 = (bf16[4,64,64]{2,1,0:T(8,128)(2,1)S(1)}, bf16[4,64,64]{2,1,0:T(8,128)(2,1)}, u32[]{:S(2)}) copy-start(bf16[4,64,64]{2,1,0:T(8,128)(2,1)} %param.19) | copy-start | bytes 98308
  58.2 76.6 %copy-start.1 = (bf16[384,2048]{1,0:T(8,128)(2,1)S(1)}, bf16[384,2048]{1,0:T(8,128)(2,1)}, u32[]{:S(2)}) copy-start(bf16[384,2048]{1,0:T(8,128)(2,1)} %param.13) | copy-start | bytes 4718596
  58.2 76.6 %copy-start.16 = (f32[2048]{0:T(1024)S(1)}, f32[2048]{0:T(1024)}, u32[]{:S(2)}) copy-start(f32[2048]{0:T(1024)} %param.14) | copy-start | bytes 24580
  59.8 80.3 %copy-start.2 = (bf16[256,1024]{1,0:T(8,128)(2,1)S(1)}, bf16[256,1024]{1,0:T(8,128)(2,1)}, u32[]{:S(2)}) copy-start(bf16[256,1024]{1,0:T(8,128)(2,1)} %param.25) | copy-start | bytes 1572868
  139.4 148.1 %all-gather.11.cloned.1.call-start = ((), (), s32[]{:S(2)}) async-start(), calls=%async_computation.5 | async-start | bytes 4718592 | tf_op jit(solution)/shard_map/all_gather | solution.py:89
  140.0 181.0 %reduce-scatter.2.cloned.1.call-start = ((), (), s32[]{:S(2)}) async-start(), calls=%async_computation.6 | async-start | bytes 1966080 | tf_op jit(solution)/shard_map/reduce_scatter | solution.py:107
  140.1 14.7 %collective-permute-start = (bf16[256,1024]{1,0:T(8,128)(2,1)S(1)}, bf16[256,1024]{1,0:T(8,128)(2,1)S(1)}, u32[]{:S(2)}, u32[]{:S(2)}) collective-permute-start(bf16[256,1024]{1,0:T(8,128)(2,1)S(1)} %copy-done.2), channel_id=1, source_target_pairs={{0,4},{4,8},{8,12},{12,16},{16,20},{20,24},{24,28},{28,0},{1,5},{5... | collective-permute-start | bytes 1572872 | tf_op jit(solution)/shard_map/ppermute | solution.py:103
  155.6 13.8 %collective-permute-start.1 = (bf16[256,1024]{1,0:T(8,128)(2,1)S(1)}, bf16[256,1024]{1,0:T(8,128)(2,1)S(1)}, u32[]{:S(2)}, u32[]{:S(2)}) collective-permute-start(bf16[256,1024]{1,0:T(8,128)(2,1)S(1)} %collective-permute-done), channel_id=1, source_target_pairs={{0,4},{4,8},{8,12},{12,16},{16,20},{20,24},{24,28},{28,0},{1,5},{5... | collective-permute-start | bytes 1572872 | tf_op jit(solution)/shard_map/ppermute | solution.py:103
  170.2 12.9 %collective-permute-start.2 = (bf16[256,1024]{1,0:T(8,128)(2,1)S(1)}, bf16[256,1024]{1,0:T(8,128)(2,1)S(1)}, u32[]{:S(2)}, u32[]{:S(2)}) collective-permute-start(bf16[256,1024]{1,0:T(8,128)(2,1)S(1)} %collective-permute-done.1), channel_id=1, source_target_pairs={{0,4},{4,8},{8,12},{12,16},{16,20},{20,24},{24,28},{28,0},{1,5},{5... | collective-permute-start | bytes 1572872 | tf_op jit(solution)/shard_map/ppermute | solution.py:103
  184.0 12.2 %collective-permute-start.3 = (bf16[256,1024]{1,0:T(8,128)(2,1)S(1)}, bf16[256,1024]{1,0:T(8,128)(2,1)S(1)}, u32[]{:S(2)}, u32[]{:S(2)}) collective-permute-start(bf16[256,1024]{1,0:T(8,128)(2,1)S(1)} %collective-permute-done.2), channel_id=1, source_target_pairs={{0,4},{4,8},{8,12},{12,16},{16,20},{20,24},{24,28},{28,0},{1,5},{5... | collective-permute-start | bytes 1572872 | tf_op jit(solution)/shard_map/ppermute | solution.py:103
  197.0 26.9 %collective-permute-start.4 = (bf16[256,1024]{1,0:T(8,128)(2,1)S(1)}, bf16[256,1024]{1,0:T(8,128)(2,1)S(1)}, u32[]{:S(2)}, u32[]{:S(2)}) collective-permute-start(bf16[256,1024]{1,0:T(8,128)(2,1)S(1)} %collective-permute-done.3), channel_id=1, source_target_pairs={{0,4},{4,8},{8,12},{12,16},{16,20},{20,24},{24,28},{28,0},{1,5},{5... | collective-permute-start | bytes 1572872 | tf_op jit(solution)/shard_map/ppermute | solution.py:103
  223.9 18.1 %copy-start.12 = (bf16[256,1024]{1,0:T(8,128)(2,1)}, bf16[256,1024]{1,0:T(8,128)(2,1)S(1)}, u32[]{:S(2)}) copy-start(bf16[256,1024]{1,0:T(8,128)(2,1)S(1)} %collective-permute-done.4) | copy-start | bytes 1572868
  223.9 18.0 %collective-permute-start.5 = (bf16[256,1024]{1,0:T(8,128)(2,1)S(1)}, bf16[256,1024]{1,0:T(8,128)(2,1)}, u32[]{:S(2)}, u32[]{:S(2)}) collective-permute-start(bf16[256,1024]{1,0:T(8,128)(2,1)S(1)} %collective-permute-done.4), channel_id=1, source_target_pairs={{0,4},{4,8},{8,12},{12,16},{16,20},{20,24},{24,28},{28,0},{1,5},{5... | collective-permute-start | bytes 1572872 | tf_op jit(solution)/shard_map/ppermute | solution.py:103
  242.0 25.6 %collective-permute-start.6 = (bf16[256,1024]{1,0:T(8,128)(2,1)}, bf16[256,1024]{1,0:T(8,128)(2,1)}, u32[]{:S(2)}, u32[]{:S(2)}) collective-permute-start(bf16[256,1024]{1,0:T(8,128)(2,1)} %collective-permute-done.5), channel_id=1, source_target_pairs={{0,4},{4,8},{8,12},{12,16},{16,20},{20,24},{24,28},{28,0},{1,5},{5... | collective-permute-start | bytes 1572872 | tf_op jit(solution)/shard_map/ppermute | solution.py:103
  242.0 29.4 %copy-start.13 = (bf16[256,1024]{1,0:T(8,128)(2,1)S(1)}, bf16[256,1024]{1,0:T(8,128)(2,1)}, u32[]{:S(2)}) copy-start(bf16[256,1024]{1,0:T(8,128)(2,1)} %copy-done.12) | copy-start | bytes 1572868
  242.0 30.2 %copy-start.11 = (bf16[256,1024]{1,0:T(8,128)(2,1)S(1)}, bf16[256,1024]{1,0:T(8,128)(2,1)}, u32[]{:S(2)}) copy-start(bf16[256,1024]{1,0:T(8,128)(2,1)} %copy-done.10) | copy-start | bytes 1572868
  244.2 32.7 %copy-start.5 = (bf16[256,1024]{1,0:T(8,128)(2,1)S(1)}, bf16[256,1024]{1,0:T(8,128)(2,1)}, u32[]{:S(2)}) copy-start(bf16[256,1024]{1,0:T(8,128)(2,1)} %copy-done.4) | copy-start | bytes 1572868
  244.3 33.5 %copy-start.3 = (bf16[256,1024]{1,0:T(8,128)(2,1)S(1)}, bf16[256,1024]{1,0:T(8,128)(2,1)}, u32[]{:S(2)}) copy-start(bf16[256,1024]{1,0:T(8,128)(2,1)} %param.25) | copy-start | bytes 1572868
  273.0 11.0 %copy-start.9 = (bf16[256,1024]{1,0:T(8,128)(2,1)S(1)}, bf16[256,1024]{1,0:T(8,128)(2,1)}, u32[]{:S(2)}) copy-start(bf16[256,1024]{1,0:T(8,128)(2,1)} %copy-done.8) | copy-start | bytes 1572868
  (7 other events, 23.5 us)
Sparse Core Ops, SparseCore 0:
  9.5 42.9 all-gather.4
  54.6 38.9 all-gather.8
  95.8 38.9 all-gather.6
  139.5 41.5 all-reduce.18
  183.1 99.0 all-gather.10
  295.7 25.2 reduce-scatter.1
